TPU v7x, 32 devices: a whole 2x2x4 slice. The times are simulated.
32 devices in a mesh: ep: 8 (over z, y), tp: 4 (over x, core).
Axes of the slice: x: 2, y: 2, z: 4, core: 2. Of those that a mesh axis runs over, the one named last changes fastest.
Arguments:
- tokens: bfloat16 [4096, 2048], P(('ep', 'tp')), may hold values from -6 to 6
- norm_gain: float32 [2048], replicated, may hold values from 0.1 to 1.9
- w_gate: bfloat16 [32, 2048, 512], P(('ep', 'tp')), may hold values from -0.125 to 0.125
- w_up: bfloat16 [32, 2048, 512], P(('ep', 'tp')), may hold values from -0.125 to 0.125
- w_down: bfloat16 [32, 512, 2048], P(('ep', 'tp')), may hold values from -0.25 to 0.25
- routing: int32 [4096, 2], P(('ep', 'tp')), may hold values from 0 to 31, as said below
- gate_weight: float32 [4096, 2], P(('ep', 'tp')), may hold values from 0.05 to 1
Outputs:
- combined: bfloat16 [4096, 2048], P(('ep', 'tp'))
Inputs may be any that keep to these rules, and one draw needn't show every extreme that they name: `routing`: A token's 2 experts are distinct and lie in one group of 4 consecutive experts. Of the 128 tokens of each device exactly 16 choose each group; no expert is named by more than 16 tokens of one device, and in every group one expert is named by exactly 16 tokens of every device.
All inputs are finite; a program needn't handle non-finite values.
Results may differ from a plain program's by a relative error of at most 0.0085.
Values may be sent and summed in bfloat16 or wider, within the bound.
A program may use at most 64 MiB of HBM per device.

v0:
```python
import jax
import jax.numpy as jnp
from jax import lax
from jax.sharding import PartitionSpec as P


def local(tokens, norm_gain, w_gate, w_up, w_down, routing, gate_weight):
    tok_rows, width = tokens.shape
    ep_count = lax.axis_size("ep")
    tp_count = lax.axis_size("tp")
    experts = ep_count * tp_count
    capacity = 4 * tok_rows // experts
    values = tokens.astype(jnp.float32)
    scale = lax.rsqrt(jnp.mean(values * values, axis=-1, keepdims=True) + 1e-06)
    normed = (values * scale * norm_gain).astype(jnp.bfloat16)
    normed_pad = jnp.concatenate([normed, jnp.zeros((1, width), jnp.bfloat16)], axis=0)
    assigned = routing.reshape(-1)
    onehot = (assigned[:, None] == jnp.arange(experts, dtype=jnp.int32)[None, :]).astype(jnp.int32)
    running = jnp.cumsum(onehot, axis=0)
    slot_index = jnp.sum(onehot * running, axis=1) - 1
    position = assigned * capacity + slot_index
    slot_owner = jnp.full((experts * capacity,), tok_rows, jnp.int32)
    slot_owner = slot_owner.at[position].set(
        jnp.arange(assigned.shape[0], dtype=jnp.int32) // routing.shape[1]
    )
    outgoing = normed_pad[slot_owner].reshape(experts, capacity, width)
    arrived = lax.all_to_all(outgoing, ("ep", "tp"), split_axis=0, concat_axis=0, tiled=True)
    slot_rows = arrived.reshape(-1, width)
    gate_part = jnp.dot(slot_rows, w_gate[0], preferred_element_type=jnp.float32)
    up_part = jnp.dot(slot_rows, w_up[0], preferred_element_type=jnp.float32)
    hidden = (jax.nn.silu(gate_part) * up_part).astype(jnp.bfloat16)
    expert_out = jnp.dot(hidden, w_down[0], preferred_element_type=jnp.float32).astype(jnp.bfloat16)
    answered = expert_out.reshape(arrived.shape)
    returned = lax.all_to_all(answered, ("ep", "tp"), split_axis=0, concat_axis=0, tiled=True)
    picked = returned.reshape(experts * capacity, width)[position]
    picked = picked.reshape(tok_rows, routing.shape[1], width).astype(jnp.float32)
    combined = jnp.sum(gate_weight[:, :, None] * picked, axis=1)
    return combined.astype(jnp.bfloat16)


def solution(mesh):
    placed = (
        P(("ep", "tp"), None),
        P(),
        P(("ep", "tp"), None, None),
        P(("ep", "tp"), None, None),
        P(("ep", "tp"), None, None),
        P(("ep", "tp"), None),
        P(("ep", "tp"), None),
    )
    return jax.shard_map(
        local, mesh=mesh, in_specs=placed, out_specs=P(("ep", "tp"), None), check_vma=False
    )
```

profile of v0, /device:TPU:0, one launch (start us, length us, event | category | flops | bytes accessed | tf_op | source)
XLA Modules:
  0.0 141.1 jit_solution(3564110494866617968)
XLA Ops:
  0.0 0.0 copy-start
  0.0 0.9 copy.11
  0.9 0.1 eq.29
  1.1 0.1 eq.25
  1.2 0.7 broadcast_multiply_fusion
  1.9 0.6 reduce-window.6
  2.5 0.2 slice_reduce_fusion
  2.7 0.1 fusion.18
  2.8 0.1 copy.10
  3.0 0.1 mul.61
  3.1 1.4 scatter_custom_fusion
  4.5 1.2 fusion.11
  5.8 1.2 fusion.13
  7.1 3.3 %gather_fusion = bf16[512,2048]{1,0:T(8,128)(2,1)} fusion(bf16[129,2048]{1,0:T(8,128)(2,1)S(1)} %concatenate.3, s32[1024]{0:T(1024)S(1)} %pad_clamp_fusion.1), kind=kCustom, calls=%fused_computation | custom fusion | bytes 4196352 | tf_op jit(solution)/shard_map/gather | solution.py:26
  10.4 0.0 copy-start.3
  10.4 56.0 %all_to_all.10 = bf16[32,16,2048]{2,1,0:T(8,128)(2,1)S(1)} all-to-all(bf16[32,16,2048]{2,1,0:T(8,128)(2,1)} %bitcast.38), channel_id=1, replica_groups=mesh['ep'=8,'tp'=4] {'ep','tp'}, dimensions={0} | all-to-all | bytes 4194304 | tf_op jit(solution)/shard_map/all_to_all | solution.py:27
  66.4 0.0 copy-start.1
  66.4 1.3 copy-done.1
  67.7 0.0 copy-done.3
  67.7 2.2 %fusion.3 = f32[512,512]{1,0:T(8,128)} fusion(bf16[512,2048]{1,0:T(8,128)(2,1)S(1)} %bitcast.40, bf16[1,2048,512]{2,1,0:T(8,128)(2,1)S(1)} %copy-done.3), kind=kOutput, calls=%fused_computation.7 | convolution fusion | flops 1073741824 | bytes 5242880 | tf_op jit(solution)/shard_map/dot_general | solution.py:29
  70.0 0.0 copy-done
  70.0 6.3 %convolution_convert_fusion = bf16[512,2048]{1,0:T(8,128)(2,1)} fusion(bf16[1,512,2048]{2,1,0:T(8,128)(2,1)S(1)} %copy-done, bf16[512,2048]{1,0:T(8,128)(2,1)} %bitcast.41, bf16[1,2048,512]{2,1,0:T(8,128)(2,1)} %param.10, f32[512,512]{1,0:T(8,128)} %fusion.3), kind=kOutput, calls=%fused_computation.3 | convolution fusion | flops 2150105088 | bytes 9437184 | tf_op jit(solution)/shard_map/dot_general | solution.py:32
  76.2 0.0 copy-start.2
  76.2 4.0 %all-to-all-start.1 = ((bf16[32,16,2048]{2,1,0:T(8,128)(2,1)}), bf16[32,16,2048]{2,1,0:T(8,128)(2,1)}, u32[]{:S(2)}, u32[]{:S(2)}) async-start(bf16[32,16,2048]{2,1,0:T(8,128)(2,1)} %bitcast.39), calls=%async_computation.1 | async-start | bytes 4194304 | tf_op jit(solution)/shard_map/all_to_all | solution.py:34
  80.2 0.0 copy-done.2
  80.2 0.1 copy.9
  80.3 48.5 %all-to-all-done.1 = bf16[32,16,2048]{2,1,0:T(8,128)(2,1)} async-done(((bf16[32,16,2048]{2,1,0:T(8,128)(2,1)}), bf16[32,16,2048]{2,1,0:T(8,128)(2,1)}, u32[]{:S(2)}, u32[]{:S(2)}) %all-to-all-start.1) | async-done | bytes 2097184 | tf_op jit(solution)/shard_map/all_to_all | solution.py:34
  128.9 4.2 %gather_fusion.1 = bf16[256,2048]{1,0:T(8,128)(2,1)S(1)} fusion(bf16[512,2048]{1,0:T(8,128)(2,1)} %bitcast.9, s32[1024]{0:T(1024)S(1)} %pad_clamp_fusion), kind=kCustom, calls=%fused_computation.1 | custom fusion | bytes 2098176 | tf_op jit(solution)/shard_map/gather | solution.py:35
  133.1 2.4 %reshape.81 = f32[128,2,2048]{2,1,0:T(2,128)} reshape(bf16[256,2048]{1,0:T(8,128)(2,1)S(1)} %gather_fusion.1) | data formatting | bytes 3145728 | tf_op jit(solution)/shard_map/convert_element_type | solution.py:36
  135.5 5.6 %multiply_reduce_fusion = bf16[128,2048]{1,0:T(8,128)(2,1)} fusion(f32[128,2,2048]{2,1,0:T(2,128)} %reshape.81, f32[128,2]{1,0:T(8,128)S(1)} %copy.9), kind=kLoop, calls=%fused_computation.9 | loop fusion | flops 786432 | bytes 2622464 | tf_op jit(solution)/shard_map/reduce_sum | solution.py:37
  (11 shorter events, 0.1 us)
Async XLA Ops:
  0.0 70.0 %copy-start = (bf16[1,512,2048]{2,1,0:T(8,128)(2,1)S(1)}, bf16[1,512,2048]{2,1,0:T(8,128)(2,1)}, u32[]{:S(2)}) copy-start(bf16[1,512,2048]{2,1,0:T(8,128)(2,1)} %param.11) | copy-start | bytes 6291460
  10.4 57.3 %copy-start.3 = (bf16[1,2048,512]{2,1,0:T(8,128)(2,1)S(1)}, bf16[1,2048,512]{2,1,0:T(8,128)(2,1)}, u32[]{:S(2)}) copy-start(bf16[1,2048,512]{2,1,0:T(8,128)(2,1)} %param.9) | copy-start | bytes 6291460
  66.4 1.3 copy-start.1
  76.2 4.0 %copy-start.2 = (f32[128,2]{0,1:T(2,128)S(1)}, f32[128,2]{0,1:T(2,128)}, u32[]{:S(2)}) copy-start(f32[128,2]{0,1:T(2,128)} %param.13) | copy-start | bytes 3076
  76.2 52.6 %all-to-all-start.1 = ((bf16[32,16,2048]{2,1,0:T(8,128)(2,1)}), bf16[32,16,2048]{2,1,0:T(8,128)(2,1)}, u32[]{:S(2)}, u32[]{:S(2)}) async-start(bf16[32,16,2048]{2,1,0:T(8,128)(2,1)} %bitcast.39), calls=%async_computation.1 | async-start | bytes 4194304 | tf_op jit(solution)/shard_map/all_to_all | solution.py:34
where the time goes:
time: 141 us
  blocking collectives  56 us (40%)
  waiting for transfers between devices  48.5 us (34%)
  local copies, waits for them, and re-layouts  14.4 us (10%)
  other arithmetic  9.5 us (7%)
  matrix products  8.49 us (6%)
  starting transfers between devices  3.98 us (3%)
    all_to_all x1, blocking collectives, local(): lax.all_to_all(outgoing, ('ep', 'tp'), split_axis=0, concat_axis=0, tiled...  56 us
    all_to_all x1, waiting for transfers between devices, local(): lax.all_to_all(answered, ('ep', 'tp'), split_axis=0, concat_axis=0, tiled...  48.5 us
    dot_general x1, matrix products, local(): jnp.dot(hidden, w_down[0], preferred_element_type=jnp.float32)  6.27 us
    reduce_sum x1, other arithmetic, local(): combined = jnp.sum(gate_weight[:, :, None] * picked, axis=1)  5.59 us
    gather x1, local copies, waits for them, and re-layouts, local(): picked = returned.reshape(experts * capacity, width)[position]  4.22 us
    all_to_all x1, starting transfers between devices, local(): lax.all_to_all(answered, ('ep', 'tp'), split_axis=0, concat_axis=0, tiled...  3.98 us
    gather x1, local copies, waits for them, and re-layouts, local(): outgoing = normed_pad[slot_owner].reshape(experts, capacity, width)  3.35 us
  transfers between devices with their start and end apart: 1, of which 1 were waited for; matrix products, arithmetic and copies ran while one was open for 0% of the time, Pallas kernels for 0%

commit v1 on v0

v1 whole, which is shorter than its diff:
```python
import functools
import jax
import jax.numpy as jnp
from jax import lax
from jax.experimental import pallas as pl
from jax.experimental.pallas import tpu as pltpu
from jax.sharding import PartitionSpec as P

BF = jnp.bfloat16
F32 = jnp.float32
MESH = pl.DeviceIdType.MESH


def flip(index, bits):
    unit = 1
    while unit <= bits:
        if bits & unit:
            index = index + unit - 2 * unit * lax.rem(lax.div(index, unit), 2)
        unit *= 2
    return index


def kernel(
    ep_count, tp_count, block, chunks,
    tok_ref, gain_ref, route_ref, gate_ref, wg_hbm, wu_hbm, wd_hbm, out_ref,
    wg, wu, wd, xcat, pack, rows_in, hid, part, pair_in, cross_out, cross_in, done, back,
    w_sem, disp_s, disp_r, core_s, core_r, x_s, x_r, fwd_s, fwd_r,
    pair_s, pair_r, cross_s, cross_r, ret_s, ret_r,
):
    toks, width = tok_ref.shape
    ff = wg.shape[1]
    slots = ep_count * block
    per = ep_count // chunks
    seg = per * block
    me_e = lax.axis_index("ep")
    me_t = lax.axis_index("tp")
    partner = {"tp": flip(me_t, 1)}
    across = {"tp": flip(me_t, 2)}
    peer = [{"ep": flip(me_e, d)} for d in range(ep_count)]

    w_copies = [
        pltpu.make_async_copy(src.at[0], dst, w_sem.at[i])
        for i, (src, dst) in enumerate(((wg_hbm, wg), (wu_hbm, wu), (wd_hbm, wd)))
    ]
    for c in w_copies:
        c.start()
    barrier = pltpu.get_barrier_semaphore()
    others = peer[1:] + [partner, across]
    for dev in others:
        pl.semaphore_signal(barrier, inc=1, device_id=dev, device_id_type=MESH)

    values = tok_ref[...].astype(F32)
    scale = lax.rsqrt(jnp.mean(values * values, axis=-1, keepdims=True) + 1e-06)
    xcat[:, :width] = (values * scale * gain_ref[...]).astype(BF)
    lane = lax.broadcasted_iota(jnp.int32, (toks, 128), 1)
    weight = jnp.zeros((toks, 128), F32)
    for k in range(route_ref.shape[1]):
        member = jnp.bitwise_and(route_ref[:, k : k + 1], tp_count - 1)
        hit = member == jnp.bitwise_and(lane, tp_count - 1)
        weight = weight + jnp.where(hit, gate_ref[:, k : k + 1], 0.0)
    hi = weight.astype(BF).astype(F32)
    mid = (weight - hi).astype(BF).astype(F32)
    low = weight - hi - mid
    tail = jnp.where(lane < tp_count, hi, jnp.where(lane < 2 * tp_count, mid, low))
    xcat[:, width:] = jnp.where(lane < 3 * tp_count, tail, 0.0).astype(BF)

    shift = tp_count.bit_length() - 1
    group = jnp.bitwise_xor(jnp.right_shift(route_ref[:, 0:1], shift), me_e)
    in_group = (group == lane).astype(F32)
    below = lax.broadcasted_iota(jnp.int32, (toks, toks), 0) > lax.broadcasted_iota(
        jnp.int32, (toks, toks), 1
    )
    ranks = jnp.dot(
        below.astype(F32).astype(BF), in_group.astype(BF), preferred_element_type=F32
    )
    rank = jnp.sum(ranks * in_group, axis=-1, keepdims=True).astype(jnp.int32)
    slot = group * block + rank
    slot_lane = lax.broadcasted_iota(jnp.int32, (toks, slots), 1)
    unpack = (slot == slot_lane).astype(F32)
    packing = unpack.T.astype(BF)
    step = min(slots, 128)
    for s in range(0, slots, step):
        pack[s : s + step, :] = jnp.dot(
            packing[s : s + step, :], xcat[...], preferred_element_type=F32
        ).astype(BF)
    rows_in[0, 0:block, :] = pack[0:block, :]

    pl.semaphore_wait(barrier, len(others))

    def remote(src, dst, s, r, dev):
        return pltpu.make_async_remote_copy(
            src_ref=src, dst_ref=dst, send_sem=s, recv_sem=r, device_id=dev, device_id_type=MESH
        )

    def place(d, pos):
        k, dd = d // per, d % per
        return rows_in.at[k, pl.ds(pos * seg + dd * block, block)]

    disp, core, xs, fwd, ret, pair, cross = {}, {}, {}, {}, {}, {}, {}
    for d in range(1, ep_count):
        disp[d] = remote(
            pack.at[pl.ds(d * block, block)], place(d, 0), disp_s.at[d], disp_r.at[d], peer[d]
        )
        disp[d].start()

    def spread(d):
        if d:
            disp[d].wait_recv()
        xs[d] = remote(place(d, 0), place(d, 1), x_s.at[d], x_r.at[d], across)
        xs[d].start()
        core[d] = remote(place(d, 0), place(d, 2), core_s.at[d], core_r.at[d], partner)
        core[d].start()

    def forward(d):
        xs[d].wait_recv()
        fwd[d] = remote(place(d, 1), place(d, 3), fwd_s.at[d], fwd_r.at[d], partner)
        fwd[d].start()

    def compute(k):
        for d in range(k * per, k * per + per):
            core[d].wait_recv()
            fwd[d].wait_recv()
        if k == 0:
            for c in w_copies:
                c.wait()
        total = tp_count * seg
        ends = lax.broadcasted_iota(jnp.int32, (total, 128), 1)
        mine = jnp.bitwise_and(ends, tp_count - 1) == me_t
        gates = jnp.sum(
            jnp.where(mine, rows_in[k, :, width:].astype(F32), 0.0), axis=-1, keepdims=True
        )
        f_tile = min(ff, 256)

        def up(j, carry):
            cols = pl.ds(pl.multiple_of(j * f_tile, f_tile), f_tile)
            rows = rows_in[k, :, :width]
            g = jnp.dot(rows, wg[:, cols], preferred_element_type=F32)
            u = jnp.dot(rows, wu[:, cols], preferred_element_type=F32)
            hid[:, cols] = (g / (1.0 + jnp.exp(-g)) * u).astype(BF)
            return carry

        lax.fori_loop(0, ff // f_tile, up, 0)
        d_tile = min(width, 512)

        def down(j, carry):
            cols = pl.ds(pl.multiple_of(j * d_tile, d_tile), d_tile)
            y = jnp.dot(hid[...], wd[:, cols], preferred_element_type=F32)
            part[k, :, cols] = (y * gates).astype(BF)
            return carry

        lax.fori_loop(0, width // d_tile, down, 0)
        pair[k] = remote(
            part.at[k, pl.ds(2 * seg, 2 * seg)], pair_in.at[k], pair_s.at[k], pair_r.at[k], partner
        )
        pair[k].start()

    def join_pair(k):
        pair[k].wait_recv()
        cross_out[k] = (
            part[k, seg : 2 * seg, :].astype(F32) + pair_in[k, seg:, :].astype(F32)
        ).astype(BF)
        cross[k] = remote(cross_out.at[k], cross_in.at[k], cross_s.at[k], cross_r.at[k], across)
        cross[k].start()

    def give_back(k):
        cross[k].wait_recv()
        done[k] = (
            part[k, 0:seg, :].astype(F32)
            + pair_in[k, 0:seg, :].astype(F32)
            + cross_in[k].astype(F32)
        ).astype(BF)
        for dd in range(per):
            d = k * per + dd
            if d == 0:
                back[0:block, :] = done[0, 0:block, :]
            else:
                ret[d] = remote(
                    done.at[k, pl.ds(dd * block, block)], back.at[pl.ds(d * block, block)],
                    ret_s.at[d], ret_r.at[d], peer[d],
                )
                ret[d].start()

    def each(f, k, lo=0, hi=None):
        for d in range(k * per + lo, k * per + (per if hi is None else hi)):
            f(d)

    half = per // 2
    each(spread, 0)
    each(forward, 0)
    each(spread, 1)
    compute(0)
    each(forward, 1)
    join_pair(0)
    compute(1)
    give_back(0)
    each(spread, 2)
    join_pair(1)
    each(forward, 2)
    give_back(1)
    compute(2)
    each(spread, 3, 0, half)
    join_pair(2)
    each(spread, 3, half)
    give_back(2)
    each(forward, 3)
    compute(3)
    join_pair(3)
    give_back(3)

    for d in range(1, ep_count):
        ret[d].wait_recv()
    out_ref[...] = jnp.dot(unpack.astype(BF), back[...], preferred_element_type=F32).astype(BF)
    for group_of in (disp, core, xs, fwd, pair, cross, ret):
        for c in group_of.values():
            c.wait_send()


def local(tokens, norm_gain, w_gate, w_up, w_down, routing, gate_weight):
    toks, width = tokens.shape
    ff = w_gate.shape[2]
    ep_count = lax.axis_size("ep")
    tp_count = lax.axis_size("tp")
    assert tp_count == 4 and ep_count % 8 == 0
    cap = toks // ep_count
    block = -(-cap // 16) * 16
    chunks = 4
    slots = ep_count * block
    seg = slots // chunks
    wide = width + 128
    vm = pl.BlockSpec(memory_space=pltpu.VMEM)
    hbm = pl.BlockSpec(memory_space=pl.ANY)
    dma = pltpu.SemaphoreType.DMA
    n_sem = [3] + [ep_count] * 8 + [chunks] * 4 + [ep_count] * 2
    return pl.pallas_call(
        functools.partial(kernel, ep_count, tp_count, block, chunks),
        out_shape=jax.ShapeDtypeStruct((toks, width), BF),
        in_specs=[vm] * 4 + [hbm] * 3,
        out_specs=vm,
        scratch_shapes=[
            pltpu.VMEM((width, ff), BF),
            pltpu.VMEM((width, ff), BF),
            pltpu.VMEM((ff, width), BF),
            pltpu.VMEM((toks, wide), BF),
            pltpu.VMEM((slots, wide), BF),
            pltpu.VMEM((chunks, tp_count * seg, wide), BF),
            pltpu.VMEM((tp_count * seg, ff), BF),
            pltpu.VMEM((chunks, tp_count * seg, width), BF),
            pltpu.VMEM((chunks, 2 * seg, width), BF),
            pltpu.VMEM((chunks, seg, width), BF),
            pltpu.VMEM((chunks, seg, width), BF),
            pltpu.VMEM((chunks, seg, width), BF),
            pltpu.VMEM((slots, width), BF),
        ] + [dma((n,)) for n in n_sem],
        compiler_params=pltpu.CompilerParams(
            collective_id=0, has_side_effects=True, vmem_limit_bytes=60 * 1024 * 1024
        ),
    )(tokens, norm_gain.reshape(1, width), routing, gate_weight, w_gate, w_up, w_down)


def solution(mesh):
    placed = (
        P(("ep", "tp"), None),
        P(),
        P(("ep", "tp"), None, None),
        P(("ep", "tp"), None, None),
        P(("ep", "tp"), None, None),
        P(("ep", "tp"), None),
        P(("ep", "tp"), None),
    )
    return jax.shard_map(
        local, mesh=mesh, in_specs=placed, out_specs=P(("ep", "tp"), None), check_vma=False
    )
```

time: 141 us -> 60.8 us (0.43)
  blocking collectives: 56 us -> 0 us
  Pallas kernels: 0 us -> 55.4 us
  waiting for transfers between devices: 48.5 us -> 0 us
  local copies, waits for them, and re-layouts: 14.4 us -> 4.7 us
  other arithmetic: 9.5 us -> 0 us
  matrix products: 8.49 us -> 0 us
  starting transfers between devices: 3.98 us -> 0 us
    all_to_all x1 -> x0, blocking collectives: 56 us -> none  [local(): lax.all_to_all(outgoing, ('ep', 'tp'), split_axis=0, concat_axis=0, tiled...]
    pallas_call x0 -> x1, Pallas kernels: none -> 55.4 us  [local(): pl.pallas_call(functools.partial(kernel, ep_count, tp_count, block, chunk...]
    all_to_all x1 -> x0, waiting for transfers between devices: 48.5 us -> none  [local(): lax.all_to_all(answered, ('ep', 'tp'), split_axis=0, concat_axis=0, tiled...]
    dot_general x2 -> x0, matrix products: 8.49 us -> none  [the longest x1 6.27 us: local(): jnp.dot(hidden, w_down[0], preferred_element_type=jnp.float32)]
    gather x2 -> x0, local copies, waits for them, and re-layouts: 7.57 us -> none  [the longest x1 4.22 us: local(): picked = returned.reshape(experts * capacity, width)[position]]
    reduce_sum x3 -> x0, other arithmetic: 6.91 us -> none  [the longest x1 5.59 us: local(): combined = jnp.sum(gate_weight[:, :, None] * picked, axis=1)]
    all_to_all x1 -> x0, starting transfers between devices: 3.98 us -> none  [local(): lax.all_to_all(answered, ('ep', 'tp'), split_axis=0, concat_axis=0, tiled...]
    convert_element_type x1 -> x0, local copies, waits for them, and re-layouts: 2.37 us -> none  [local(): picked.reshape(tok_rows, routing.shape[1], width).astype(jnp.float32)]
  transfers between devices with their start and end apart: 1 -> 0, of which waited for: 1 -> 0; matrix products, arithmetic and copies ran while one was open for 0% -> 0% of each run, Pallas kernels for 0% -> 0%
where the time goes in v1:
time: 60.8 us; the launch traced here: 60.1 us
  Pallas kernels  55.4 us (91%)
  local copies, waits for them, and re-layouts  4.7 us (8%)
    pallas_call x1, Pallas kernels, local(): pl.pallas_call(functools.partial(kernel, ep_count, tp_count, block, chunk...  55.4 us
    unnamed x3, local copies, waits for them, and re-layouts  4.7 us

profile of v1, /device:TPU:0, one launch (start us, length us, event | category | flops | bytes accessed | tf_op | source)
XLA Modules:
  0.0 60.1 jit_solution(3696284761307635575)
XLA Ops:
  0.0 1.4 %copy.8.route_ref = s32[128,2]{1,0:T(8,128)} copy(s32[128,2]{0,1:T(2,128)} %param.12) | data formatting | bytes 2048 | tf_op args[5]
  1.4 1.4 %copy.9.gate_ref = f32[128,2]{1,0:T(8,128)} copy(f32[128,2]{0,1:T(2,128)} %param.13) | data formatting | bytes 2048 | tf_op args[6]
  2.8 55.4 %shard_map.73 = bf16[128,2048]{1,0:T(8,128)(2,1)} custom-call(bf16[128,2048]{1,0:T(8,128)(2,1)} %tok_ref.1, f32[1,2048]{1,0:T(1,128)} %bitcast.1, s32[128,2]{1,0:T(8,128)} %copy.8.route_ref, f32[128,2]{1,0:T(8,128)} %copy.9.gate_ref, bf16[1,2048,512]{2,1,0:T(8,128)(2,1)} %wg_hbm.1, bf16[1,2048,512]{2,1,0:T(8,128)(2,1)} %wu_hbm.1, bf16[1,512,2048]{2,1,0:T(8,128)(2,1)} %wd_hbm.1), custom_call_target="tpu_custom_call" | custom-call | tf_op jit(solution)/shard_map/pallas_call | solution.py:234
  58.2 1.9 %copy.11 = bf16[128,2048]{1,0:T(8,128)(2,1)} copy(bf16[128,2048]{1,0:T(8,128)(2,1)} %shard_map.73) | data formatting | bytes 1048576

commit v2 on v1

v2 whole, which is shorter than its diff:
```python
import functools
import jax
import jax.numpy as jnp
from jax import lax
from jax.experimental import pallas as pl
from jax.experimental.pallas import tpu as pltpu
from jax.sharding import PartitionSpec as P

BF = jnp.bfloat16
F32 = jnp.float32
MESH = pl.DeviceIdType.MESH

SENT = (0, 1, 4, 2, 5, 3, 6, 7)
CUTS = (0, 2, 4, 6, 7, 8)
ORDER = "s0 s1 s2 s3 f0 f1 c0 s4 f2 f3 j0 c1 s5 j1 f4 g0 s6 f5 c2 s7 g1 j2 f6 c3 g2 f7 j3 c4 j4 g3 g4"


def flip(index, bits):
    unit = 1
    while unit <= bits:
        if bits & unit:
            index = index + unit - 2 * unit * lax.rem(lax.div(index, unit), 2)
        unit *= 2
    return index


def kernel(
    ep_count, tp_count, block, cuts,
    tok_ref, gain_ref, route_ref, gate_ref, wg_hbm, wu_hbm, wd_hbm, out_ref,
    wg, wu, wd, xcat, pack, rows_in, hid, part, pair_in, cross_out, cross_in, done, back,
    w_sem, disp_s, disp_r, core_s, core_r, x_s, x_r, fwd_s, fwd_r,
    pair_s, pair_r, cross_s, cross_r, ret_s, ret_r,
):
    toks, width = tok_ref.shape
    ff = wg.shape[1]
    slots = ep_count * block
    chunk_of = {}
    for k in range(len(cuts) - 1):
        for d in range(cuts[k], cuts[k + 1]):
            chunk_of[d] = k
    me_e = lax.axis_index("ep")
    me_t = lax.axis_index("tp")
    partner = {"tp": flip(me_t, 1)}
    across = {"tp": flip(me_t, 2)}
    peer = [{"ep": flip(me_e, d)} for d in range(ep_count)]

    w_copies = [
        pltpu.make_async_copy(src.at[0], dst, w_sem.at[i])
        for i, (src, dst) in enumerate(((wg_hbm, wg), (wu_hbm, wu), (wd_hbm, wd)))
    ]
    for c in w_copies:
        c.start()
    barrier = pltpu.get_barrier_semaphore()
    others = peer[1:] + [partner, across]
    for dev in others:
        pl.semaphore_signal(barrier, inc=1, device_id=dev, device_id_type=MESH)

    shift = tp_count.bit_length() - 1
    group = jnp.bitwise_xor(jnp.right_shift(route_ref[0:1, :], shift), me_e)
    heads = -(-ep_count // 16) * 16
    in_group = (lax.broadcasted_iota(jnp.int32, (heads, toks), 0) == group).astype(F32)
    above = lax.broadcasted_iota(jnp.int32, (toks, toks), 0) < lax.broadcasted_iota(
        jnp.int32, (toks, toks), 1
    )
    ranks = jnp.dot(
        in_group.astype(BF), above.astype(F32).astype(BF), preferred_element_type=F32
    )
    rank = jnp.sum(ranks * in_group, axis=0, keepdims=True).astype(jnp.int32)
    slot = group * block + rank
    packing = (lax.broadcasted_iota(jnp.int32, (slots, toks), 0) == slot).astype(F32)

    line = lax.broadcasted_iota(jnp.int32, (128, toks), 0)
    weight = jnp.zeros((128, toks), F32)
    for k in range(route_ref.shape[0]):
        member = jnp.bitwise_and(route_ref[k : k + 1, :], tp_count - 1)
        hit = jnp.bitwise_and(line, tp_count - 1) == member
        weight = weight + jnp.where(hit, gate_ref[k : k + 1, :], 0.0)
    hi = weight.astype(BF).astype(F32)
    mid = (weight - hi).astype(BF).astype(F32)
    low = weight - hi - mid
    tail = jnp.where(line < tp_count, hi, jnp.where(line < 2 * tp_count, mid, low))
    xcat[:, width:] = jnp.where(line < 3 * tp_count, tail, 0.0).T.astype(BF)
    values = tok_ref[...].astype(F32)
    scale = lax.rsqrt(jnp.mean(values * values, axis=-1, keepdims=True) + 1e-06)
    xcat[:, :width] = (values * scale * gain_ref[...]).astype(BF)
    step = min(slots, 128)
    for s in range(0, slots, step):
        pack[s : s + step, :] = jnp.dot(
            packing[s : s + step, :].astype(BF), xcat[...], preferred_element_type=F32
        ).astype(BF)
    rows_in[0:block, :] = pack[0:block, :]

    pl.semaphore_wait(barrier, len(others))

    def remote(src, dst, s, r, dev):
        return pltpu.make_async_remote_copy(
            src_ref=src, dst_ref=dst, send_sem=s, recv_sem=r, device_id=dev, device_id_type=MESH
        )

    def span(k):
        return cuts[k] * block, (cuts[k + 1] - cuts[k]) * block

    def place(d, pos):
        base, seg = span(chunk_of[d])
        return rows_in.at[pl.ds(4 * base + pos * seg + d * block - base, block)]

    disp, core, xs, fwd, ret, pair, cross = {}, {}, {}, {}, {}, {}, {}
    unit = ep_count // 8
    sent = [n * unit + i for n in SENT for i in range(unit)]
    for d in [d for d in sent if d]:
        disp[d] = remote(
            pack.at[pl.ds(d * block, block)], place(d, 0), disp_s.at[d], disp_r.at[d], peer[d]
        )
        disp[d].start()

    def spread(d):
        if d:
            disp[d].wait_recv()
        xs[d] = remote(place(d, 0), place(d, 1), x_s.at[d], x_r.at[d], across)
        xs[d].start()
        core[d] = remote(place(d, 0), place(d, 2), core_s.at[d], core_r.at[d], partner)
        core[d].start()

    def forward(d):
        xs[d].wait_recv()
        fwd[d] = remote(place(d, 1), place(d, 3), fwd_s.at[d], fwd_r.at[d], partner)
        fwd[d].start()

    def compute(k):
        for d in range(cuts[k], cuts[k + 1]):
            core[d].wait_recv()
            fwd[d].wait_recv()
        if k == first:
            for c in w_copies:
                c.wait()
        base, seg = span(k)
        total = tp_count * seg
        start = tp_count * base
        ends = lax.broadcasted_iota(jnp.int32, (total, 128), 1)
        mine = jnp.bitwise_and(ends, tp_count - 1) == me_t
        gates = jnp.sum(
            jnp.where(mine, rows_in[start : start + total, width:].astype(F32), 0.0),
            axis=-1, keepdims=True,
        )
        f_tile = min(ff, 256)

        def up(j, carry):
            cols = pl.ds(pl.multiple_of(j * f_tile, f_tile), f_tile)
            rows = rows_in[start : start + total, :width]
            g = jnp.dot(rows, wg[:, cols], preferred_element_type=F32)
            u = jnp.dot(rows, wu[:, cols], preferred_element_type=F32)
            hid[:total, cols] = (g / (1.0 + jnp.exp(-g)) * u).astype(BF)
            return carry

        lax.fori_loop(0, ff // f_tile, up, 0)
        d_tile = min(width, 512)

        def down(j, carry):
            cols = pl.ds(pl.multiple_of(j * d_tile, d_tile), d_tile)
            y = jnp.dot(hid[:total, :], wd[:, cols], preferred_element_type=F32)
            part[start : start + total, cols] = (y * gates).astype(BF)
            return carry

        lax.fori_loop(0, width // d_tile, down, 0)
        pair[k] = remote(
            part.at[pl.ds(start + 2 * seg, 2 * seg)], pair_in.at[pl.ds(2 * base, 2 * seg)],
            pair_s.at[k], pair_r.at[k], partner,
        )
        pair[k].start()

    def join_pair(k):
        base, seg = span(k)
        start = tp_count * base
        pair[k].wait_recv()
        cross_out[base : base + seg, :] = (
            part[start + seg : start + 2 * seg, :].astype(F32)
            + pair_in[2 * base + seg : 2 * base + 2 * seg, :].astype(F32)
        ).astype(BF)
        cross[k] = remote(
            cross_out.at[pl.ds(base, seg)], cross_in.at[pl.ds(base, seg)],
            cross_s.at[k], cross_r.at[k], across,
        )
        cross[k].start()

    def give_back(k):
        base, seg = span(k)
        start = tp_count * base
        cross[k].wait_recv()
        done[base : base + seg, :] = (
            part[start : start + seg, :].astype(F32)
            + pair_in[2 * base : 2 * base + seg, :].astype(F32)
            + cross_in[base : base + seg, :].astype(F32)
        ).astype(BF)
        for d in range(cuts[k], cuts[k + 1]):
            if d == 0:
                back[0:block, :] = done[0:block, :]
            else:
                at = pl.ds(d * block, block)
                ret[d] = remote(done.at[at], back.at[at], ret_s.at[d], ret_r.at[d], peer[d])
                ret[d].start()

    steps = ORDER.split()
    first = int(next(s for s in steps if s[0] == "c")[1:])
    for name in steps:
        number = int(name[1:])
        if name[0] in "sf":
            for d in range(number * unit, number * unit + unit):
                (spread if name[0] == "s" else forward)(d)
        else:
            {"c": compute, "j": join_pair, "g": give_back}[name[0]](number)

    for d in range(1, ep_count):
        ret[d].wait_recv()
    out_ref[...] = jnp.dot(packing.T.astype(BF), back[...], preferred_element_type=F32).astype(BF)
    for group_of in (disp, core, xs, fwd, pair, cross, ret):
        for c in group_of.values():
            c.wait_send()


def local(tokens, norm_gain, w_gate, w_up, w_down, routing, gate_weight):
    toks, width = tokens.shape
    ff = w_gate.shape[2]
    ep_count = lax.axis_size("ep")
    tp_count = lax.axis_size("tp")
    assert tp_count == 4 and ep_count % 8 == 0
    cap = toks // ep_count
    block = -(-cap // 16) * 16
    cuts = [c * (ep_count // 8) for c in CUTS]
    chunks = len(cuts) - 1
    slots = ep_count * block
    most = max(b - a for a, b in zip(cuts, cuts[1:])) * block * tp_count
    wide = width + 128
    vm = pl.BlockSpec(memory_space=pltpu.VMEM)
    hbm = pl.BlockSpec(memory_space=pl.ANY)
    dma = pltpu.SemaphoreType.DMA
    n_sem = [3] + [ep_count] * 8 + [chunks] * 4 + [ep_count] * 2
    return pl.pallas_call(
        functools.partial(kernel, ep_count, tp_count, block, cuts),
        out_shape=jax.ShapeDtypeStruct((toks, width), BF),
        in_specs=[vm] * 4 + [hbm] * 3,
        out_specs=vm,
        scratch_shapes=[
            pltpu.VMEM((width, ff), BF),
            pltpu.VMEM((width, ff), BF),
            pltpu.VMEM((ff, width), BF),
            pltpu.VMEM((toks, wide), BF),
            pltpu.VMEM((slots, wide), BF),
            pltpu.VMEM((tp_count * slots, wide), BF),
            pltpu.VMEM((most, ff), BF),
            pltpu.VMEM((tp_count * slots, width), BF),
            pltpu.VMEM((2 * slots, width), BF),
            pltpu.VMEM((slots, width), BF),
            pltpu.VMEM((slots, width), BF),
            pltpu.VMEM((slots, width), BF),
            pltpu.VMEM((slots, width), BF),
        ] + [dma((n,)) for n in n_sem],
        compiler_params=pltpu.CompilerParams(
            collective_id=0, has_side_effects=True, vmem_limit_bytes=60 * 1024 * 1024
        ),
    )(tokens, norm_gain.reshape(1, width), routing.T, gate_weight.T, w_gate, w_up, w_down)


def solution(mesh):
    placed = (
        P(("ep", "tp"), None),
        P(),
        P(("ep", "tp"), None, None),
        P(("ep", "tp"), None, None),
        P(("ep", "tp"), None, None),
        P(("ep", "tp"), None),
        P(("ep", "tp"), None),
    )
    return jax.shard_map(
        local, mesh=mesh, in_specs=placed, out_specs=P(("ep", "tp"), None), check_vma=False
    )
```

time: 60.8 us -> 49.5 us (0.81)
  Pallas kernels: 55.4 us -> 47 us
  local copies, waits for them, and re-layouts: 4.7 us -> 1.88 us
    pallas_call x1, Pallas kernels: 55.4 us -> 47 us  [local(): pl.pallas_call(functools.partial(kernel, ep_count, tp_count, block, cuts)...]
    unnamed x3 -> x1, local copies, waits for them, and re-layouts: 4.7 us -> 1.88 us
where the time goes in v2:
time: 49.5 us; the launch traced here: 48.9 us
  Pallas kernels  47 us (95%)
  local copies, waits for them, and re-layouts  1.88 us (4%)
    pallas_call x1, Pallas kernels, local(): pl.pallas_call(functools.partial(kernel, ep_count, tp_count, block, cuts)...  47 us
    unnamed x1, local copies, waits for them, and re-layouts  1.88 us

profile of v2, /device:TPU:0, one launch (start us, length us, event | category | flops | bytes accessed | tf_op | source)
XLA Modules:
  0.0 48.9 jit_solution(6352660722612143273)
XLA Ops:
  0.0 47.0 %shard_map.73 = bf16[128,2048]{1,0:T(8,128)(2,1)} custom-call(bf16[128,2048]{1,0:T(8,128)(2,1)} %tok_ref.1, f32[1,2048]{1,0:T(1,128)} %bitcast.3, s32[2,128]{1,0:T(2,128)} %bitcast.4, f32[2,128]{1,0:T(2,128)} %bitcast.5, bf16[1,2048,512]{2,1,0:T(8,128)(2,1)} %wg_hbm.1, bf16[1,2048,512]{2,1,0:T(8,128)(2,1)} %wu_hbm.1, bf16[1,512,2048]{2,1,0:T(8,128)(2,1)} %wd_hbm.1), custom_call_target="tpu_custom_call" | custom-call | tf_op jit(solution)/shard_map/pallas_call | solution.py:237
  47.0 1.9 %copy.9 = bf16[128,2048]{1,0:T(8,128)(2,1)} copy(bf16[128,2048]{1,0:T(8,128)(2,1)} %shard_map.73) | data formatting | bytes 1048576
